TPU v7x, 32 devices: a whole 2x2x4 slice. The times are simulated.
32 devices in a mesh: grp: 2 (over y), ep: 4 (over z), tp: 4 (over x, core).
Axes of the slice: x: 2, y: 2, z: 4, core: 2. Of those that a mesh axis runs over, the one named last changes fastest.
Arguments:
- query_first: bfloat16 [3072, 512], P(('grp', 'ep'), 'tp'), parts along dimension 0, may hold values from -32 to 32
- query_second: bfloat16 [3072, 512], P(('grp', 'ep'), 'tp'), parts along dimension 0, may hold values from -32 to 32
- key_first: bfloat16 [3072, 512], P(('grp', 'ep'), 'tp'), parts along dimension 0, may hold values from -32 to 32
- key_second: bfloat16 [3072, 512], P(('grp', 'ep'), 'tp'), parts along dimension 0, may hold values from -32 to 32
- values: bfloat16 [3072, 1024], P(('grp', 'ep'), 'tp'), parts along dimension 0, may hold values from -6 to 6
- lambda_head: float32 [8], P('tp'), may hold values from 0.3 to 0.8
- head_gain: float32 [128], replicated, may hold values from 0.1 to 1.9
- out_weight: bfloat16 [1024, 2048], replicated, may hold values from -0.1875 to 0.1875
- tokens: bfloat16 [4096, 2048], P(('grp', 'ep', 'tp')), parts along dimension 0, may hold values from -6 to 6
- norm_gain: float32 [2048], replicated, may hold values from 0.1 to 1.9
- expert_ids: int32 [4096, 2], P(('grp', 'ep', 'tp')), parts along dimension 0, may hold values from 0 to 3, all different within a row; in each aligned block of 128 rows (0 to 127, 128 to 255, ...) at most 96 rows name the same one
- expert_weights: float32 [4096, 2], P(('grp', 'ep', 'tp')), parts along dimension 0, may hold values from 0.2 to 1
- expert_gate: bfloat16 [4, 2048, 1024], P('ep', None, 'tp'), may hold values from -0.125 to 0.125
- expert_up: bfloat16 [4, 2048, 1024], P('ep', None, 'tp'), may hold values from -0.125 to 0.125
- expert_down: bfloat16 [4, 1024, 2048], P('ep', 'tp'), may hold values from -0.1875 to 0.1875
- shared_gate: bfloat16 [2048, 512], P(None, 'tp'), may hold values from -0.125 to 0.125
- shared_up: bfloat16 [2048, 512], P(None, 'tp'), may hold values from -0.125 to 0.125
- shared_down: bfloat16 [512, 2048], P('tp'), may hold values from -0.25 to 0.25
Outputs:
- mixed: bfloat16 [3072, 2048], P(('grp', 'ep', 'tp')), parts along dimension 0
- expert_out: bfloat16 [4096, 2048], P(('grp', 'ep', 'tp')), parts along dimension 0
There are 2 independent parts, one for each index of `grp`. A program takes and returns all parts, laid end to end along the dimension named above; an argument that names none is the same for every part. Nothing has to cross between parts.
Inputs may be any that keep to these rules, and one draw needn't show every extreme that they name: `expert_ids`: in the rows of one device (aligned blocks of 128 rows) no expert is named by more than 96 rows, and in every draw some expert is named by exactly 96 rows of some block; each row names 2 different experts.
All inputs are finite; a program needn't handle non-finite values.
Results may differ from a plain program's by a relative error of at most 0.012.
Values may be sent and summed in bfloat16 or wider, within the bound.
A program may use at most 128 MiB of HBM per device.

v0:
```python
import jax
import jax.numpy as jnp
from jax import lax
from jax.sharding import PartitionSpec as P

epsilon = 1e-06
block_limit = 1536


def key_block(total_rows, shard_rows):
    if total_rows <= block_limit or total_rows % shard_rows != 0:
        return total_rows
    best_rows = shard_rows
    for factor_rows in range(1, total_rows // shard_rows + 1):
        if total_rows % (factor_rows * shard_rows) == 0 and factor_rows * shard_rows <= block_limit:
            best_rows = factor_rows * shard_rows
    return best_rows


def softmax_update(states, scores, value_block):
    running_max, running_sum, accumulated = states
    new_max = jnp.maximum(running_max, jnp.max(scores, axis=-1))
    rescale = jnp.exp(running_max - new_max)
    weights = jnp.exp(scores - new_max[..., None])
    new_sum = running_sum * rescale + jnp.sum(weights, axis=-1)
    product = jnp.einsum(
        "qhk,khe->qhe",
        weights.astype(jnp.bfloat16),
        value_block,
        preferred_element_type=jnp.float32,
    )
    return (new_max, new_sum, accumulated * rescale[..., None] + product)


def shards(
    query_first,
    query_second,
    key_first,
    key_second,
    values,
    lambda_head,
    head_gain,
    out_weight,
    tokens,
    norm_gain,
    expert_ids,
    expert_weights,
    expert_gate,
    expert_up,
    expert_down,
    shared_gate,
    shared_up,
    shared_down,
):
    shard_rows, query_width = query_first.shape
    heads_here = lambda_head.shape[0]
    head_size = query_width // heads_here
    value_size = values.shape[1] // heads_here
    score_scale = head_size ** (-0.5)
    query_one = query_first.reshape(shard_rows, heads_here, head_size)
    query_two = query_second.reshape(shard_rows, heads_here, head_size)
    initial = (
        jnp.full((shard_rows, heads_here), -jnp.inf, jnp.float32),
        jnp.zeros((shard_rows, heads_here), jnp.float32),
        jnp.zeros((shard_rows, heads_here, value_size), jnp.float32),
    )
    carried = (initial, initial)
    key_one = lax.all_gather(key_first, "ep", axis=0, tiled=True)
    key_two = lax.all_gather(key_second, "ep", axis=0, tiled=True)
    value_piece = lax.all_gather(values, "ep", axis=0, tiled=True)
    total_rows = key_one.shape[0]
    block_rows = key_block(total_rows, shard_rows)
    block_count = total_rows // block_rows
    stacked = (
        key_one.reshape(block_count, block_rows, heads_here, head_size),
        key_two.reshape(block_count, block_rows, heads_here, head_size),
        value_piece.reshape(block_count, block_rows, heads_here, value_size),
    )

    def fold_step(states, blocks):
        first_state, second_state = states
        key_a, key_b, value_block = blocks
        scores_a = (
            jnp.einsum("qhd,khd->qhk", query_one, key_a, preferred_element_type=jnp.float32)
            * score_scale
        )
        scores_b = (
            jnp.einsum("qhd,khd->qhk", query_two, key_b, preferred_element_type=jnp.float32)
            * score_scale
        )
        return (
            (
                softmax_update(first_state, scores_a, value_block),
                softmax_update(second_state, scores_b, value_block),
            ),
            None,
        )

    carried, unused = lax.scan(fold_step, carried, stacked)
    first_state, second_state = carried
    first_out = first_state[2] / first_state[1][..., None]
    second_out = second_state[2] / second_state[1][..., None]
    mixture = first_out - lambda_head[None, :, None] * second_out
    normed_heads = (
        mixture
        * lax.rsqrt(jnp.mean(mixture * mixture, axis=-1, keepdims=True) + epsilon)
        * head_gain
    )
    head_local = normed_heads.astype(jnp.bfloat16).reshape(shard_rows, heads_here * value_size)
    position_heads = lax.all_to_all(head_local, "tp", split_axis=0, concat_axis=1, tiled=True)
    mixed = jnp.dot(position_heads, out_weight, preferred_element_type=jnp.float32).astype(
        jnp.bfloat16
    )
    row_count, model_width = tokens.shape
    top_count = expert_ids.shape[1]
    ep_count = lax.axis_size("ep")
    local_experts = expert_gate.shape[0]
    expert_count = local_experts * ep_count
    capacity = max(2, row_count * top_count * 3 // (2 * expert_count))
    routed_rows = expert_count * capacity
    owner_span = routed_rows + row_count
    widened = tokens.astype(jnp.float32)
    normed = (
        widened
        * lax.rsqrt(jnp.mean(widened * widened, axis=-1, keepdims=True) + epsilon)
        * norm_gain
    ).astype(jnp.bfloat16)
    flat_ids = expert_ids.reshape(-1)
    onehot = (flat_ids[:, None] == jnp.arange(expert_count, dtype=jnp.int32)[None, :]).astype(
        jnp.int32
    )
    ranks = jnp.sum(onehot * jnp.cumsum(onehot, axis=0), axis=1) - 1
    slot_index = flat_ids * capacity + ranks
    token_index = jnp.arange(flat_ids.shape[0], dtype=jnp.int32) // top_count
    filled = jnp.full((routed_rows,), row_count, jnp.int32).at[slot_index].set(token_index)
    padded = jnp.concatenate([normed, jnp.zeros((1, model_width), jnp.bfloat16)], axis=0)
    outgoing = padded[filled].reshape(1, ep_count, local_experts * capacity, model_width)
    arrived = lax.all_to_all(outgoing, "ep", split_axis=1, concat_axis=1, tiled=True)
    local_rows = jnp.concatenate(
        [arrived.reshape(1, routed_rows, model_width), normed[None]], axis=1
    )
    gathered = lax.all_gather(local_rows, "tp", axis=0, tiled=True)
    owners = owner_span * lax.axis_size("tp") // owner_span
    routed_in = gathered[:, :routed_rows].reshape(
        owners, ep_count, local_experts, capacity, model_width
    )
    gate_value = jnp.einsum(
        "osecd,edf->osecf", routed_in, expert_gate, preferred_element_type=jnp.float32
    )
    up_value = jnp.einsum(
        "osecd,edf->osecf", routed_in, expert_up, preferred_element_type=jnp.float32
    )
    hidden = (jax.nn.silu(gate_value) * up_value).astype(jnp.bfloat16)
    routed_out = jnp.einsum(
        "osecf,efd->osecd", hidden, expert_down, preferred_element_type=jnp.float32
    )
    routed_out = routed_out.reshape(owners, routed_rows, model_width)
    shared_in = gathered[:, routed_rows:]
    shared_gate_value = jnp.einsum(
        "ord,df->orf", shared_in, shared_gate, preferred_element_type=jnp.float32
    )
    shared_up_value = jnp.einsum(
        "ord,df->orf", shared_in, shared_up, preferred_element_type=jnp.float32
    )
    shared_hidden = (jax.nn.silu(shared_gate_value) * shared_up_value).astype(jnp.bfloat16)
    shared_out = jnp.einsum(
        "orf,fd->ord", shared_hidden, shared_down, preferred_element_type=jnp.float32
    )
    kept_rows = lax.psum_scatter(
        jnp.concatenate([routed_out, shared_out], axis=1)
        .reshape(owners * owner_span, model_width)
        .astype(jnp.bfloat16),
        "tp",
        scatter_dimension=0,
        tiled=True,
    ).astype(jnp.float32)
    routed_back = (
        kept_rows[:routed_rows]
        .astype(jnp.bfloat16)
        .reshape(ep_count, local_experts * capacity, model_width)
    )
    returned = lax.all_to_all(routed_back, "ep", split_axis=0, concat_axis=0, tiled=True).reshape(
        routed_rows, model_width
    )
    picked = returned[slot_index].reshape(row_count, top_count, model_width).astype(jnp.float32)
    combined = jnp.sum(picked * expert_weights[:, :, None], axis=1) + kept_rows[routed_rows:]
    expert_out = combined.astype(jnp.bfloat16)
    return (mixed, expert_out)


def solution(mesh):
    placed = (
        P(("grp", "ep"), "tp"),
        P(("grp", "ep"), "tp"),
        P(("grp", "ep"), "tp"),
        P(("grp", "ep"), "tp"),
        P(("grp", "ep"), "tp"),
        P("tp"),
        P(),
        P(),
        P(("grp", "ep", "tp"), None),
        P(),
        P(("grp", "ep", "tp"), None),
        P(("grp", "ep", "tp"), None),
        P("ep", None, "tp"),
        P("ep", None, "tp"),
        P("ep", "tp", None),
        P(None, "tp"),
        P(None, "tp"),
        P("tp", None),
    )
    return jax.shard_map(
        shards,
        mesh=mesh,
        in_specs=placed,
        out_specs=(P(("grp", "ep", "tp"), None), P(("grp", "ep", "tp"), None)),
        check_vma=False,
    )
```

profile of v0, /device:TPU:8, one launch (start us, length us, event | category | flops | bytes accessed | tf_op | source)
XLA Modules:
  0.0 287.2 jit_solution(5120199368730788813)
XLA Ops:
  14.9 3.1 %gather_fusion = bf16[384,2048]{1,0:T(8,128)(2,1)} fusion(bf16[129,2048]{1,0:T(8,128)(2,1)S(1)} %concatenate.10, s32[1024]{0:T(1024)S(1)} %pad_clamp_fusion.1), kind=kCustom, calls=%fused_computation | custom fusion | bytes 3147264 | tf_op jit(solution)/shard_map/gather | solution.py:137
  18.1 5.3 %all-to-all-start.1 = ((bf16[1,4,96,2048]{3,2,0,1:T(8,128)(2,1)}), bf16[1,4,96,2048]{3,2,0,1:T(8,128)(2,1)S(1)}, u32[]{:S(2)}, u32[]{:S(2)}) async-start(bf16[1,4,96,2048]{3,2,0,1:T(8,128)(2,1)} %bitcast.182), calls=%async_computation.1 | async-start | bytes 3145728 | tf_op jit(solution)/shard_map/all_to_all | solution.py:138
  24.4 32.7 %all-to-all-done.1 = bf16[1,4,96,2048]{3,2,0,1:T(8,128)(2,1)S(1)} async-done(((bf16[1,4,96,2048]{3,2,0,1:T(8,128)(2,1)}), bf16[1,4,96,2048]{3,2,0,1:T(8,128)(2,1)S(1)}, u32[]{:S(2)}, u32[]{:S(2)}) %all-to-all-start.1) | async-done | bytes 1572896 | tf_op jit(solution)/shard_map/all_to_all | solution.py:138
  57.1 2.6 pad_maximum_fusion.1
  59.9 60.0 %all-gather.2.cloned.1.call-done = bf16[4,512,2048]{2,1,0:T(8,128)(2,1)} async-done(((bf16[1,512,2048]{2,1,0:T(8,128)(2,1)}), bf16[4,512,2048]{2,1,0:T(8,128)(2,1)}) %all-gather.2.cloned.1.call-update) | async-done | bytes 8388624 | tf_op jit(solution)/shard_map/all_gather | solution.py:142
  120.0 3.4 %slice.34 = bf16[4,384,2048]{2,1,0:T(8,128)(2,1)S(1)} slice(bf16[4,512,2048]{2,1,0:T(8,128)(2,1)} %all-gather.2.cloned.1.call-done), slice={[0:4], [0:384], [0:2048]} | slice | bytes 12582912 | tf_op jit(solution)/shard_map/slice | solution.py:144
  123.3 2.6 copy-done.2
  125.9 3.0 %fusion.61 = f32[4,4,96,256]{3,2,1,0:T(8,128)} fusion(bf16[4,4,96,2048]{3,2,1,0:T(8,128)(2,1)S(1)} %bitcast.177, bf16[1,2048,256]{2,1,0:T(8,128)(2,1)S(1)} %copy-done.12), kind=kOutput, calls=%fused_computation.54 | convolution fusion | flops 1610612736 | bytes 8912896 | tf_op jit(solution)/shard_map/osecd,edf->osecf/dot_general | solution.py:147
  128.9 12.4 %convolution_convert_fusion = bf16[4,4,96,2048]{3,2,1,0:T(8,128)(2,1)} fusion(bf16[4,4,96,2048]{3,2,1,0:T(8,128)(2,1)} %bitcast.178, f32[4,4,96,256]{3,2,1,0:T(8,128)} %fusion.61, bf16[1,256,2048]{2,1,0:T(8,128)(2,1)S(1)} %copy-done, bf16[1,2048,256]{2,1,0:T(8,128)(2,1)S(1)} %copy-done.13), kind=kOutput, calls=%fused_computation.10 | convolution fusion | flops 3226730496 | bytes 16252928 | tf_op jit(solution)/shard_map/osecf,efd->osecd/dot_general | solution.py:154
  141.4 2.3 fusion.16
  143.7 4.1 %convolution_convert_fusion.1 = bf16[4,128,2048]{2,1,0:T(8,128)(2,1)S(1)} fusion(bf16[4,512,2048]{2,1,0:T(8,128)(2,1)} %all-gather.2.cloned.1.call-done, bf16[128,2048]{1,0:T(8,128)(2,1)} %param.35, bf16[2048,128]{1,0:T(8,128)(2,1)} %param.34, f32[4,128,128]{2,1,0:T(8,128)S(1)} %fusion.16), kind=kOutput, calls=%fused_computation.15 | convolution fusion | flops 538312704 | bytes 5505024 | tf_op jit(solution)/shard_map/orf,fd->ord/dot_general | solution.py:166
  147.8 7.6 %pad_maximum_fusion = bf16[4,512,2048]{2,1,0:T(8,128)(2,1)} fusion(bf16[4,128,2048]{2,1,0:T(8,128)(2,1)S(1)} %convolution_convert_fusion.1, bf16[4,384,2048]{2,1,0:T(8,128)(2,1)} %bitcast.181), kind=kLoop, calls=%fused_computation.3 | loop fusion | flops 16777216 | bytes 16777216 | tf_op jit(solution)/shard_map/concatenate | solution.py:170
  156.4 18.1 %all_gather.13 = bf16[1536,256]{1,0:T(8,128)(2,1)S(1)} all-gather(bf16[384,256]{1,0:T(8,128)(2,1)S(1)} %copy-done.4), channel_id=1, replica_groups=mesh['grp'=2,'ep'=4,'tp'=4] {'ep'}, dimensions={0}, use_global_device_ids=true | all-gather | bytes 983040 | tf_op jit(solution)/shard_map/all_gather | solution.py:70
  174.7 15.5 %all_gather.14 = bf16[1536,128]{1,0:T(8,128)(2,1)S(1)} all-gather(bf16[384,128]{1,0:T(8,128)(2,1)S(1)} %copy-done.7), channel_id=1, replica_groups=mesh['grp'=2,'ep'=4,'tp'=4] {'ep'}, dimensions={0}, use_global_device_ids=true | all-gather | bytes 491520 | tf_op jit(solution)/shard_map/all_gather | solution.py:69
  190.6 14.8 %all_gather.12 = bf16[1536,128]{1,0:T(8,128)(2,1)S(1)} all-gather(bf16[384,128]{1,0:T(8,128)(2,1)S(1)} %copy-done.8), channel_id=1, replica_groups=mesh['grp'=2,'ep'=4,'tp'=4] {'ep'}, dimensions={0}, use_global_device_ids=true | all-gather | bytes 491520 | tf_op jit(solution)/shard_map/all_gather | solution.py:68
  212.2 3.4 %all-to-all-start = ((bf16[4,96,256]{2,1,0:T(8,128)(2,1)}), bf16[4,96,256]{2,1,0:T(8,128)(2,1)S(1)}, u32[]{:S(2)}, u32[]{:S(2)}) async-start(bf16[4,96,256]{2,1,0:T(8,128)(2,1)} %all_to_all.20), calls=%async_computation | async-start | bytes 393216 | tf_op jit(solution)/shard_map/all_to_all | solution.py:110
  215.6 13.6 %reduce-scatter.2.cloned.1.call-done = bf16[512,2048]{1,0:T(8,128)(2,1)} async-done(((bf16[2048,2048]{1,0:T(8,128)(2,1)}), bf16[512,2048]{1,0:T(8,128)(2,1)}) %reduce-scatter.2.cloned.1.call-update) | async-done | bytes 2097168 | tf_op jit(solution)/shard_map/reduce_scatter | solution.py:169
  229.1 2.7 slice.36
  231.9 5.1 %all-to-all-start.2 = ((bf16[4,96,2048]{2,1,0:T(8,128)(2,1)}), bf16[4,96,2048]{2,1,0:T(8,128)(2,1)S(1)}, u32[]{:S(2)}, u32[]{:S(2)}) async-start(bf16[4,96,2048]{2,1,0:T(8,128)(2,1)} %bitcast.179), calls=%async_computation.3 | async-start | bytes 3145728 | tf_op jit(solution)/shard_map/all_to_all | solution.py:182
  237.2 3.7 %convolution_convert_fusion.2 = bf16[96,2048]{1,0:T(8,128)(2,1)} fusion(bf16[96,1024]{1,0:T(8,128)(2,1)S(1)} %bitcast.185, bf16[1024,2048]{1,0:T(8,128)(2,1)} %param.25), kind=kOutput, calls=%fused_computation.22 | convolution fusion | flops 402849792 | bytes 4784128 | tf_op jit(solution)/shard_map/dot_general | solution.py:111
  240.9 29.6 %all-to-all-done.2 = bf16[4,96,2048]{2,1,0:T(8,128)(2,1)S(1)} async-done(((bf16[4,96,2048]{2,1,0:T(8,128)(2,1)}), bf16[4,96,2048]{2,1,0:T(8,128)(2,1)S(1)}, u32[]{:S(2)}, u32[]{:S(2)}) %all-to-all-start.2) | async-done | bytes 1572896 | tf_op jit(solution)/shard_map/all_to_all | solution.py:182
  270.5 2.3 gather_fusion.1
  272.9 2.4 reshape.171
  275.3 3.2 %multiply_reduce_fusion = f32[128,2048]{1,0:T(8,128)S(1)} fusion(f32[128,2,2048]{2,1,0:T(2,128)S(1)} %reshape.171, f32[128,2]{1,0:T(8,128)S(1)} %copy.60), kind=kLoop, calls=%fused_computation.24 | loop fusion | flops 786432 | bytes 3146752 | tf_op jit(solution)/shard_map/reduce_sum | solution.py:186
  (83 shorter events, 19.2 us)
Async XLA Ops:
  7.2 121.8 %copy-start = (bf16[1,256,2048]{2,1,0:T(8,128)(2,1)S(1)}, bf16[1,256,2048]{2,1,0:T(8,128)(2,1)}, u32[]{:S(2)}) copy-start(bf16[1,256,2048]{2,1,0:T(8,128)(2,1)} %param.32) | copy-start | bytes 3145732
  14.9 8.5 %copy-start.3 = (bf16[128,2048]{1,0:T(8,128)(2,1)S(1)}, bf16[128,2048]{1,0:T(8,128)(2,1)}, u32[]{:S(2)}) copy-start(bf16[128,2048]{1,0:T(8,128)(2,1)} %param.26) | copy-start | bytes 1572868
  14.9 8.5 %copy-start.9 = (f32[2048]{0:T(1024)S(1)}, f32[2048]{0:T(1024)}, u32[]{:S(2)}) copy-start(f32[2048]{0:T(1024)} %param.27) | copy-start | bytes 24580
  18.1 39.0 %all-to-all-start.1 = ((bf16[1,4,96,2048]{3,2,0,1:T(8,128)(2,1)}), bf16[1,4,96,2048]{3,2,0,1:T(8,128)(2,1)S(1)}, u32[]{:S(2)}, u32[]{:S(2)}) async-start(bf16[1,4,96,2048]{3,2,0,1:T(8,128)(2,1)} %bitcast.182), calls=%async_computation.1 | async-start | bytes 3145728 | tf_op jit(solution)/shard_map/all_to_all | solution.py:138
  23.4 96.6 %all-gather.2.cloned.1.call-start = ((), (), s32[]{:S(2)}) async-start(), calls=%async_computation.4 | async-start | bytes 10485760 | tf_op jit(solution)/shard_map/all_gather | solution.py:142
  59.7 66.2 %copy-start.12 = (bf16[1,2048,256]{2,1,0:T(8,128)(2,1)S(1)}, bf16[1,2048,256]{2,1,0:T(8,128)(2,1)}, u32[]{:S(2)}) copy-start(bf16[1,2048,256]{2,1,0:T(8,128)(2,1)} %param.30) | copy-start | bytes 3145732
  59.7 169.4 %reduce-scatter.2.cloned.1.call-start = ((), (), s32[]{:S(2)}) async-start(), calls=%async_computation.5 | async-start | bytes 10485760 | tf_op jit(solution)/shard_map/reduce_scatter | solution.py:169
  123.3 2.6 copy-start.2
  125.9 3.1 %copy-start.13 = (bf16[1,2048,256]{2,1,0:T(8,128)(2,1)S(1)}, bf16[1,2048,256]{2,1,0:T(8,128)(2,1)}, u32[]{:S(2)}) copy-start(bf16[1,2048,256]{2,1,0:T(8,128)(2,1)} %param.31) | copy-start | bytes 3145732
  128.9 12.4 %copy-start.14 = (bf16[2048,128]{1,0:T(8,128)(2,1)S(1)}, bf16[2048,128]{1,0:T(8,128)(2,1)}, u32[]{:S(2)}) copy-start(bf16[2048,128]{1,0:T(8,128)(2,1)} %param.33) | copy-start | bytes 1572868
  155.4 0.9 copy-start.4
  155.4 19.3 %copy-start.7 = (bf16[384,128]{1,0:T(8,128)(2,1)S(1)}, bf16[384,128]{1,0:T(8,128)(2,1)}, u32[]{:S(2)}) copy-start(bf16[384,128]{1,0:T(8,128)(2,1)} %param.21) | copy-start | bytes 294916
  155.4 35.0 %copy-start.5 = (bf16[384,128]{1,0:T(8,128)(2,1)S(1)}, bf16[384,128]{1,0:T(8,128)(2,1)}, u32[]{:S(2)}) copy-start(bf16[384,128]{1,0:T(8,128)(2,1)} %param.19) | copy-start | bytes 294916
  155.4 35.2 %copy-start.8 = (bf16[384,128]{1,0:T(8,128)(2,1)S(1)}, bf16[384,128]{1,0:T(8,128)(2,1)}, u32[]{:S(2)}) copy-start(bf16[384,128]{1,0:T(8,128)(2,1)} %param.20) | copy-start | bytes 294916
  156.3 49.3 %copy-start.6 = (bf16[384,128]{1,0:T(8,128)(2,1)S(1)}, bf16[384,128]{1,0:T(8,128)(2,1)}, u32[]{:S(2)}) copy-start(bf16[384,128]{1,0:T(8,128)(2,1)} %param.18) | copy-start | bytes 294916
  207.4 1.7 copy-start.15
  210.1 1.0 copy-start.11
  211.1 26.0 %copy-start.10 = (f32[128,2]{0,1:T(2,128)S(1)}, f32[128,2]{0,1:T(2,128)}, u32[]{:S(2)}) copy-start(f32[128,2]{0,1:T(2,128)} %param.29) | copy-start | bytes 3076
  212.2 19.7 %all-to-all-start = ((bf16[4,96,256]{2,1,0:T(8,128)(2,1)}), bf16[4,96,256]{2,1,0:T(8,128)(2,1)S(1)}, u32[]{:S(2)}, u32[]{:S(2)}) async-start(bf16[4,96,256]{2,1,0:T(8,128)(2,1)} %all_to_all.20), calls=%async_computation | async-start | bytes 393216 | tf_op jit(solution)/shard_map/all_to_all | solution.py:110
  231.9 38.7 %all-to-all-start.2 = ((bf16[4,96,2048]{2,1,0:T(8,128)(2,1)}), bf16[4,96,2048]{2,1,0:T(8,128)(2,1)S(1)}, u32[]{:S(2)}, u32[]{:S(2)}) async-start(bf16[4,96,2048]{2,1,0:T(8,128)(2,1)} %bitcast.179), calls=%async_computation.3 | async-start | bytes 3145728 | tf_op jit(solution)/shard_map/all_to_all | solution.py:182
  270.5 9.9 %copy-start.1 = (bf16[1,256,2048]{2,1,0:T(8,128)(2,1)S(1)}, bf16[1,256,2048]{2,1,0:T(8,128)(2,1)}, u32[]{:S(2)}) copy-start(bf16[1,256,2048]{2,1,0:T(8,128)(2,1)} %param.32) | copy-start | bytes 3145732
Sparse Core Ops, SparseCore 0:
  59.8 60.0 all-gather.1
  155.6 73.5 reduce-scatter.1
where the time goes:
time: 292 us; the launch traced here: 287 us
  waiting for transfers between devices  136 us (47%)
  blocking collectives  48.5 us (17%)
  matrix products  29.3 us (10%)
  other arithmetic  22.7 us (8%)
  local copies, waits for them, and re-layouts  22.5 us (8%)
  between operations  14.4 us (5%)
  starting transfers between devices  14 us (5%)
    all_gather x1, waiting for transfers between devices, shards(): gathered = lax.all_gather(local_rows, 'tp', axis=0, tiled=True)  60 us
    all_to_all x1, waiting for transfers between devices, shards(): lax.all_to_all(outgoing, 'ep', split_axis=1, concat_axis=1, tiled=True)  32.7 us
    all_to_all x1, waiting for transfers between devices, shards(): lax.all_to_all(routed_back, 'ep', split_axis=0, concat_axis=0, tiled=True)  29.6 us
    all_gather x1, blocking collectives, shards(): value_piece = lax.all_gather(values, 'ep', axis=0, tiled=True)  18.1 us
    all_gather x1, blocking collectives, shards(): key_two = lax.all_gather(key_second, 'ep', axis=0, tiled=True)  15.5 us
    all_gather x1, blocking collectives, shards(): key_one = lax.all_gather(key_first, 'ep', axis=0, tiled=True)  14.8 us
    reduce_scatter x1, waiting for transfers between devices, shards(): lax.psum_scatter(jnp.concatenate([routed_out, shared_out], axis=1).reshap...  13.6 us
    dot_general x1, matrix products, shards(): jnp.einsum('osecf,efd->osecd', hidden, expert_down, preferred_element_typ...  12.4 us
  transfers between devices with their start and end apart: 5, of which 4 were waited for; matrix products, arithmetic and copies ran while one was open for 5% of the time, Pallas kernels for 0%

commit v1 on v0

--- a/solution.py
+++ b/solution.py
@@ -1,6 +1,9 @@
 import jax
 import jax.numpy as jnp
 from jax import lax
+from jax.experimental import pallas as pl
+from jax.experimental.pallas import tpu as pltpu
+import functools
 from jax.sharding import PartitionSpec as P
 
 epsilon = 1e-06
@@ -188,6 +191,514 @@
     return (mixed, expert_out)
 
 
+MESH = pl.DeviceIdType.MESH
+BF = jnp.bfloat16
+F32 = jnp.float32
+
+
+def fused_fits(mesh):
+    return mesh.shape["ep"] == 4 and mesh.shape["tp"] == 4
+
+
+def fused_kernel(
+    zn,
+    tokens_ref,
+    gain_ref,
+    wloc_ref,
+    qa_ref,
+    qb_ref,
+    ka_hbm,
+    kb_hbm,
+    v_hbm,
+    lam_ref,
+    hgain_ref,
+    gate_hbm,
+    up_hbm,
+    down_hbm,
+    sgate_hbm,
+    sup_hbm,
+    sdown_hbm,
+    wo_hbm,
+    mixed_ref,
+    out_ref,
+    gbuf,
+    wbuf,
+    kbuf,
+    pbuf,
+    abuf,
+    bbuf,
+    cbuf,
+    hout,
+    hbuf,
+    gate,
+    up,
+    down,
+    sgate,
+    sup,
+    sdown,
+    wo,
+    lsem,
+    gsend,
+    grecv,
+    wsend,
+    wrecv,
+    ksend,
+    krecv,
+    asend,
+    arecv,
+    bsend,
+    brecv,
+    csend,
+    crecv,
+    hsend,
+    hrecv,
+):
+    grp = lax.axis_index("grp")
+    z = lax.axis_index("ep")
+    t = lax.axis_index("tp")
+    c = lax.rem(t, 2)
+    x = lax.div(t, 2)
+    partner = 2 * x + 1 - c
+    peer = 2 * (1 - x) + c
+    diag = 2 * (1 - x) + 1 - c
+    tn = 4
+    rows = tokens_ref.shape[0]
+    width = tokens_ref.shape[1]
+    arow = qa_ref.shape[0]
+    kw = ka_hbm.shape[1]
+    vw = v_hbm.shape[1]
+
+    has_up = z < zn - 1
+    has_dn = z > 0
+    up_dev = (grp, jnp.minimum(z + 1, zn - 1), t)
+    dn_dev = (grp, jnp.maximum(z - 1, 0), t)
+    partner_dev = (grp, z, partner)
+    peer_dev = (grp, z, peer)
+
+    loads = [
+        pltpu.make_async_copy(ka_hbm, kbuf.at[z, :, pl.ds(0, kw)], lsem.at[0]),
+        pltpu.make_async_copy(kb_hbm, kbuf.at[z, :, pl.ds(kw, kw)], lsem.at[1]),
+        pltpu.make_async_copy(v_hbm, kbuf.at[z, :, pl.ds(2 * kw, vw)], lsem.at[2]),
+        pltpu.make_async_copy(gate_hbm.at[0], gate, lsem.at[3]),
+        pltpu.make_async_copy(up_hbm.at[0], up, lsem.at[4]),
+        pltpu.make_async_copy(down_hbm.at[0], down, lsem.at[5]),
+        pltpu.make_async_copy(sgate_hbm, sgate, lsem.at[6]),
+        pltpu.make_async_copy(sup_hbm, sup, lsem.at[7]),
+        pltpu.make_async_copy(sdown_hbm, sdown, lsem.at[8]),
+        pltpu.make_async_copy(wo_hbm, wo, lsem.at[9]),
+    ]
+    for load in loads:
+        load.start()
+
+    barrier = pltpu.get_barrier_semaphore()
+    for other in (partner, peer, diag):
+        pl.semaphore_signal(barrier, inc=1, device_id=(grp, z, other), device_id_type=MESH)
+
+    @pl.when(has_up)
+    def _():
+        pl.semaphore_signal(barrier, inc=1, device_id=up_dev, device_id_type=MESH)
+
+    @pl.when(has_dn)
+    def _():
+        pl.semaphore_signal(barrier, inc=1, device_id=dn_dev, device_id_type=MESH)
+
+    own = z * tn + t
+    wide = tokens_ref[...].astype(F32)
+    scale = lax.rsqrt(jnp.mean(wide * wide, axis=-1, keepdims=True) + epsilon)
+    gbuf[own] = (wide * scale * gain_ref[...]).astype(BF)
+    wbuf[own] = wloc_ref[...]
+
+    pl.semaphore_wait(barrier, 3 + jnp.where(has_up, 1, 0) + jnp.where(has_dn, 1, 0))
+
+    def remote(src, dst, ssem, rsem, dev):
+        return pltpu.make_async_remote_copy(
+            src_ref=src, dst_ref=dst, send_sem=ssem, recv_sem=rsem, device_id=dev, device_id_type=MESH
+        )
+
+    def gcopies(slot, way, dev):
+        return (
+            remote(gbuf.at[slot], gbuf.at[slot], gsend.at[way, slot], grecv.at[slot], dev),
+            remote(wbuf.at[slot], wbuf.at[slot], wsend.at[way, slot], wrecv.at[slot], dev),
+        )
+
+    def gstart(slot, way, dev):
+        for one in gcopies(slot, way, dev):
+            one.start()
+
+    def gwait_recv(slot):
+        for one in gcopies(slot, 0, partner_dev):
+            one.wait_recv()
+
+    def gwait_send(slot, way, dev):
+        for one in gcopies(slot, way, dev):
+            one.wait_send()
+
+    def goes_up(k):
+        return jnp.logical_and(has_up, k <= z)
+
+    def goes_down(k):
+        return jnp.logical_and(has_dn, k >= z)
+
+    def order(j):
+        low = jnp.minimum(z, zn - 1 - z)
+        first = jnp.where(j < 2, 1 - j, j)
+        near = jnp.where(low == 1, first, j)
+        return jnp.where(z < 2, near, zn - 1 - near)
+
+    def forward(k):
+        slot = k * tn + t
+
+        @pl.when(goes_up(k))
+        def _():
+            gstart(slot, 0, up_dev)
+
+        @pl.when(goes_down(k))
+        def _():
+            gstart(slot, 1, dn_dev)
+
+        gstart(slot, 2, peer_dev)
+        gstart(slot, 3, partner_dev)
+
+    forward(z)
+    inner = jnp.minimum(z, zn - 1 - z)
+
+    def kcopy(k, way, dev):
+        return remote(kbuf.at[k], kbuf.at[k], ksend.at[way, k], krecv.at[k], dev)
+
+    def kforward(k):
+        @pl.when(goes_up(k))
+        def _():
+            kcopy(k, 0, up_dev).start()
+
+        @pl.when(goes_down(k))
+        def _():
+            kcopy(k, 1, dn_dev).start()
+
+    def acopy(k, xd):
+        return remote(
+            pbuf.at[k, 2 * xd + 1 - c], abuf.at[k, xd], asend.at[k, xd], arecv.at[k, xd], partner_dev
+        )
+
+    for load in loads[3:9]:
+        load.wait()
+
+    def silu_mul(g, u):
+        return (g * (1.0 / (1.0 + jnp.exp(-g))) * u).astype(BF)
+
+    def gather_step(j, carry):
+        for i in range(1, 4):
+            when = jnp.where(inner == 1, max(i - 2, 0), i - 1)
+
+            @pl.when(j == when)
+            def _():
+                k = order(i)
+                gwait_recv(k * tn + t)
+                forward(k)
+                if i == 3:
+                    for load in loads[:3]:
+                        load.wait()
+                    kforward(z)
+
+        k = order(j)
+        gwait_recv(k * tn + peer)
+        gstart(k * tn + peer, 3, partner_dev)
+        gwait_recv(k * tn + partner)
+        gwait_recv(k * tn + diag)
+        rows_in = gbuf[pl.ds(k * tn, tn)].reshape(tn * rows, width)
+        g = jnp.dot(rows_in, gate[...], preferred_element_type=F32)
+        u = jnp.dot(rows_in, up[...], preferred_element_type=F32)
+        hidden = silu_mul(g, u)
+        pieces = []
+        for s in range(tn):
+            turned = wbuf[k * tn + s].T
+            lane = lax.broadcasted_iota(jnp.int32, turned.shape, 1)
+            pieces.append(jnp.sum(jnp.where(lane == z, turned, 0.0), axis=1, keepdims=True))
+        weight = jnp.concatenate(pieces, axis=0)
+        half = width // 2
+        for h in range(2):
+            cols = pl.ds(h * half, half)
+            part = jnp.dot(hidden, down[:, h * half : (h + 1) * half], preferred_element_type=F32)
+            pbuf[k, :, :, cols] = (part * weight).astype(BF).reshape(tn, rows, half)
+
+        @pl.when(j == 0)
+        def _():
+            sg = jnp.dot(rows_in, sgate[...], preferred_element_type=F32)
+            su = jnp.dot(rows_in, sup[...], preferred_element_type=F32)
+            sh = silu_mul(sg, su)
+            for h in range(2):
+                cols = pl.ds(h * half, half)
+                part = jnp.dot(sh, sdown[:, h * half : (h + 1) * half], preferred_element_type=F32)
+                before = pbuf[k, :, :, cols].astype(F32)
+                pbuf[k, :, :, cols] = (before + part.reshape(tn, rows, half)).astype(BF)
+
+        for xd in range(2):
+            acopy(k, xd).start()
+        return carry
+
+    lax.fori_loop(0, zn, gather_step, 0)
+
+    def bcopy(k):
+        return remote(pbuf.at[k, peer], bbuf.at[k], bsend.at[k], brecv.at[k], peer_dev)
+
+    def pair_step(i, carry):
+        k = order(zn - 1 - i)
+        acopy(k, 0).wait_recv()
+        acopy(k, 1).wait_recv()
+        pbuf[k, peer] = (pbuf[k, peer].astype(F32) + abuf[k, 1 - x].astype(F32)).astype(BF)
+        bcopy(k).start()
+        pbuf[k, t] = (pbuf[k, t].astype(F32) + abuf[k, x].astype(F32)).astype(BF)
+        return carry
+
+    lax.fori_loop(0, zn, pair_step, 0)
+
+    def key_step(j, carry):
+        k = order(j)
+        kcopy(k, 0, partner_dev).wait_recv()
+        kforward(k)
+        return carry
+
+    lax.fori_loop(1, zn, key_step, 0)
+
+    heads = vw // hgain_ref.shape[1]
+    head = kw // heads
+    vdim = vw // heads
+    qrows = arow // 3
+
+    def attend_step(i, carry):
+        r = pl.multiple_of(i * qrows, qrows)
+        for h in range(heads):
+            lane = lax.broadcasted_iota(jnp.int32, (qrows, kw), 1)
+            mine = jnp.logical_and(lane >= h * head, lane < (h + 1) * head)
+            outs = []
+            for m, q_ref in enumerate((qa_ref, qb_ref)):
+                q = jnp.where(mine, q_ref[pl.ds(r, qrows), :], jnp.zeros((), BF))
+                keys = kbuf[:, :, m * kw : (m + 1) * kw].reshape(zn * arow, kw)
+                s = lax.dot_general(q, keys, (((1,), (1,)), ((), ())), preferred_element_type=F32)
+                s = s * (head ** -0.5)
+                peak = jnp.max(s, axis=-1, keepdims=True)
+                e = jnp.exp(s - peak)
+                total = jnp.sum(e, axis=-1, keepdims=True)
+                vals = kbuf[:, :, 2 * kw + h * vdim : 2 * kw + (h + 1) * vdim].reshape(zn * arow, vdim)
+                o = jnp.dot(e.astype(BF), vals, preferred_element_type=F32)
+                outs.append(o / total)
+            mix = outs[0] - lam_ref[0, h] * outs[1]
+            norm = lax.rsqrt(jnp.mean(mix * mix, axis=-1, keepdims=True) + epsilon)
+            hout[pl.ds(r, qrows), h * vdim : (h + 1) * vdim] = (mix * norm * hgain_ref[...]).astype(BF)
+        return carry
+
+    lax.fori_loop(0, 3, attend_step, 0)
+
+    orow = arow // tn
+
+    def hcopy(to):
+        return remote(
+            hout.at[pl.ds(pl.multiple_of(to * orow, 16), orow), :],
+            hbuf.at[t],
+            hsend.at[to],
+            hrecv.at[t],
+            (grp, z, to),
+        )
+
+    def hrecv_wait(src):
+        remote(
+            hout.at[pl.ds(0, orow), :], hbuf.at[src], hsend.at[src], hrecv.at[src], (grp, z, src)
+        ).wait_recv()
+
+    for other in (peer, diag, partner):
+        hcopy(other).start()
+    hbuf[t] = hout[pl.ds(pl.multiple_of(t * orow, 16), orow), :]
+
+    def ccopy(k, way, dev):
+        return remote(pbuf.at[k, t], cbuf.at[way, k], csend.at[k], crecv.at[way, k], dev)
+
+    def line_step(i, carry):
+        k = order(zn - 1 - i)
+        bcopy(k).wait_recv()
+        pbuf[k, t] = (pbuf[k, t].astype(F32) + bbuf[k].astype(F32)).astype(BF)
+
+        @pl.when(k > z)
+        def _():
+            @pl.when(has_dn)
+            def _():
+                ccopy(k, 0, up_dev).wait_recv()
+                pbuf[k, t] = (pbuf[k, t].astype(F32) + cbuf[0, k].astype(F32)).astype(BF)
+
+            ccopy(k, 0, up_dev).start()
+
+        @pl.when(k < z)
+        def _():
+            @pl.when(has_up)
+            def _():
+                ccopy(k, 1, dn_dev).wait_recv()
+                pbuf[k, t] = (pbuf[k, t].astype(F32) + cbuf[1, k].astype(F32)).astype(BF)
+
+            ccopy(k, 1, dn_dev).start()
+
+        return carry
+
+    lax.fori_loop(0, zn - 1, line_step, 0)
+
+    for other in (partner, peer, diag):
+        hrecv_wait(other)
+    loads[9].wait()
+    half = width // 2
+    for h in range(2):
+        acc = jnp.zeros((orow, half), F32)
+        for s in range(tn):
+            acc = acc + jnp.dot(
+                hbuf[s], wo[s * vw : (s + 1) * vw, h * half : (h + 1) * half], preferred_element_type=F32
+            )
+        mixed_ref[:, h * half : (h + 1) * half] = acc.astype(BF)
+
+    bcopy(z).wait_recv()
+    pbuf[z, t] = (pbuf[z, t].astype(F32) + bbuf[z].astype(F32)).astype(BF)
+
+    @pl.when(has_dn)
+    def _():
+        ccopy(z, 0, up_dev).wait_recv()
+        pbuf[z, t] = (pbuf[z, t].astype(F32) + cbuf[0, z].astype(F32)).astype(BF)
+
+    @pl.when(has_up)
+    def _():
+        ccopy(z, 1, dn_dev).wait_recv()
+        pbuf[z, t] = (pbuf[z, t].astype(F32) + cbuf[1, z].astype(F32)).astype(BF)
+
+    out_ref[...] = pbuf[z, t]
+
+    def drain_step(k, carry):
+        slot = k * tn + t
+
+        @pl.when(goes_up(k))
+        def _():
+            gwait_send(slot, 0, up_dev)
+            kcopy(k, 0, up_dev).wait_send()
+
+        @pl.when(goes_down(k))
+        def _():
+            gwait_send(slot, 1, dn_dev)
+            kcopy(k, 1, dn_dev).wait_send()
+
+        gwait_send(slot, 2, peer_dev)
+        gwait_send(slot, 3, partner_dev)
+        gwait_send(k * tn + peer, 3, partner_dev)
+        for xd in range(2):
+            acopy(k, xd).wait_send()
+        bcopy(k).wait_send()
+
+        @pl.when(k != z)
+        def _():
+            ccopy(k, 0, up_dev).wait_send()
+
+        return carry
+
+    lax.fori_loop(0, zn, drain_step, 0)
+    for other in (partner, peer, diag):
+        hcopy(other).wait_send()
+
+
+def fused_shards(
+    zn,
+    query_first,
+    query_second,
+    key_first,
+    key_second,
+    values,
+    lambda_head,
+    head_gain,
+    out_weight,
+    tokens,
+    norm_gain,
+    expert_ids,
+    expert_weights,
+    expert_gate,
+    expert_up,
+    expert_down,
+    shared_gate,
+    shared_up,
+    shared_down,
+):
+    rows, width = tokens.shape
+    arow, kw = key_first.shape
+    vw = values.shape[1]
+    tn = lax.axis_size("tp")
+    pad = 8
+    names = jnp.arange(pad, dtype=jnp.int32)[:, None]
+    wloc = jnp.zeros((pad, rows), F32)
+    for top in range(expert_ids.shape[1]):
+        wloc = wloc + jnp.where(expert_ids[:, top][None, :] == names, expert_weights[:, top][None, :], 0.0)
+    vmem = pl.BlockSpec(memory_space=pltpu.VMEM)
+    smem = pl.BlockSpec(memory_space=pltpu.SMEM)
+    hbm = pl.BlockSpec(memory_space=pltpu.HBM)
+    dma = pltpu.SemaphoreType.DMA
+    slots = zn * tn
+    hidden = expert_gate.shape[2]
+    shared = shared_gate.shape[1]
+    mixed, expert_out = pl.pallas_call(
+        functools.partial(fused_kernel, zn),
+        out_shape=(
+            jax.ShapeDtypeStruct((arow // tn, width), BF),
+            jax.ShapeDtypeStruct((rows, width), BF),
+        ),
+        in_specs=[vmem, vmem, vmem, vmem, vmem, hbm, hbm, hbm, smem, vmem] + [hbm] * 7,
+        out_specs=(vmem, vmem),
+        scratch_shapes=[
+            pltpu.VMEM((slots, rows, width), BF),
+            pltpu.VMEM((slots, pad, rows), F32),
+            pltpu.VMEM((zn, arow, 2 * kw + vw), BF),
+            pltpu.VMEM((zn, tn, rows, width), BF),
+            pltpu.VMEM((zn, 2, rows, width), BF),
+            pltpu.VMEM((zn, rows, width), BF),
+            pltpu.VMEM((2, zn, rows, width), BF),
+            pltpu.VMEM((arow, vw), BF),
+            pltpu.VMEM((tn, arow // tn, vw), BF),
+            pltpu.VMEM((width, hidden), BF),
+            pltpu.VMEM((width, hidden), BF),
+            pltpu.VMEM((hidden, width), BF),
+            pltpu.VMEM((width, shared), BF),
+            pltpu.VMEM((width, shared), BF),
+            pltpu.VMEM((shared, width), BF),
+            pltpu.VMEM(out_weight.shape, BF),
+            dma((10,)),
+            dma((4, slots)),
+            dma((slots,)),
+            dma((4, slots)),
+            dma((slots,)),
+            dma((2, zn)),
+            dma((zn,)),
+            dma((zn, 2)),
+            dma((zn, 2)),
+            dma((zn,)),
+            dma((zn,)),
+            dma((zn,)),
+            dma((2, zn)),
+            dma((tn,)),
+            dma((tn,)),
+        ],
+        compiler_params=pltpu.CompilerParams(
+            collective_id=0, has_side_effects=True, vmem_limit_bytes=66000000
+        ),
+    )(
+        tokens,
+        norm_gain[None, :],
+        wloc,
+        query_first,
+        query_second,
+        key_first,
+        key_second,
+        values,
+        lambda_head[None, :],
+        head_gain[None, :],
+        expert_gate,
+        expert_up,
+        expert_down,
+        shared_gate,
+        shared_up,
+        shared_down,
+        out_weight,
+    )
+    return mixed, expert_out
+
+
 def solution(mesh):
     placed = (
         P(("grp", "ep"), "tp"),
@@ -209,8 +720,9 @@
         P(None, "tp"),
         P("tp", None),
     )
+    body = functools.partial(fused_shards, mesh.shape["ep"]) if fused_fits(mesh) else shards
     return jax.shard_map(
-        shards,
+        body,
         mesh=mesh,
         in_specs=placed,
         out_specs=(P(("grp", "ep", "tp"), None), P(("grp", "ep", "tp"), None)),

time: 292 us -> 129 us (0.44)
  waiting for transfers between devices: 136 us -> 0 us
  Pallas kernels: 0 us -> 120 us
  blocking collectives: 48.5 us -> 0 us
  matrix products: 29.3 us -> 0 us
  other arithmetic: 22.7 us -> 0.6 us
  local copies, waits for them, and re-layouts: 22.5 us -> 5.16 us
  starting transfers between devices: 14 us -> 0 us
  between operations: 14.4 us -> 0.64 us
    pallas_call x0 -> x1, Pallas kernels: none -> 120 us  [fused_shards(): pl.pallas_call(functools.partial(fused_kernel, zn), out_shape=(jax.ShapeD...]
    all_to_all x3 -> x0, waiting for transfers between devices: 62.3 us -> none  [the longest x1 32.7 us: shards(): lax.all_to_all(outgoing, 'ep', split_axis=1, concat_axis=1, tiled=True)]
    all_gather x1 -> x0, waiting for transfers between devices: 60 us -> none  [shards(): gathered = lax.all_gather(local_rows, 'tp', axis=0, tiled=True)]
    all_gather x3 -> x0, blocking collectives: 48.5 us -> none  [the longest x1 18.1 us: shards(): value_piece = lax.all_gather(values, 'ep', axis=0, tiled=True)]
    dot_general x9 -> x0, matrix products: 29.3 us -> none  [the longest x1 12.4 us: shards(): jnp.einsum('osecf,efd->osecd', hidden, expert_down, preferred_element_typ...]
    all_to_all x3 -> x0, starting transfers between devices: 13.8 us -> none  [the longest x1 5.32 us: shards(): lax.all_to_all(outgoing, 'ep', split_axis=1, concat_axis=1, tiled=True)]
    reduce_scatter x1 -> x0, waiting for transfers between devices: 13.6 us -> none  [shards(): lax.psum_scatter(jnp.concatenate([routed_out, shared_out], axis=1).reshap...]
    concatenate x2 -> x0, other arithmetic: 10.2 us -> none  [the longest x1 7.61 us: shards(): jnp.concatenate([routed_out, shared_out], axis=1)]
  transfers between devices with their start and end apart: 5 -> 0, of which waited for: 4 -> 0; matrix products, arithmetic and copies ran while one was open for 5% -> 0% of each run, Pallas kernels for 0% -> 0%
where the time goes in v1:
time: 129 us; the launch traced here: 126 us
  Pallas kernels  120 us (93%)
  local copies, waits for them, and re-layouts  5.16 us (4%)
    pallas_call x1, Pallas kernels, fused_shards(): pl.pallas_call(functools.partial(fused_kernel, zn), out_shape=(jax.ShapeD...  120 us
    unnamed x2, local copies, waits for them, and re-layouts  3.65 us

profile of v1, /device:TPU:8, one launch (start us, length us, event | category | flops | bytes accessed | tf_op | source)
XLA Modules:
  0.0 126.4 jit_solution(16321436330232609376)
XLA Ops:
  0.6 0.8 slice_bitcast_fusion.3
  1.4 0.8 slice_bitcast_fusion.2
  2.1 0.6 select_add_fusion.wloc_ref
  2.7 120.0 %shard_map.185 = (bf16[96,2048]{1,0:T(8,128)(2,1)}, bf16[128,2048]{1,0:T(8,128)(2,1)}) custom-call(bf16[128,2048]{1,0:T(8,128)(2,1)} %tokens_ref.1, f32[1,2048]{1,0:T(1,128)} %bitcast.11, f32[8,128]{1,0:T(8,128)} %select_add_fusion.wloc_ref, bf16[384,128]{1,0:T(8,128)(2,1)} %qa_ref.1, bf16[384,128]{1,0:T(8,128)(2,1)} %qb_ref.1, bf16[384,128]{1,0:T(8,128)(2,1)} %ka_hbm.1, ...), custom_call_target="tpu_custom_call" | custom-call | tf_op jit(solution)/shard_map/pallas_call | solution.py:636
  122.8 1.8 %copy.22 = bf16[96,2048]{1,0:T(8,128)(2,1)} copy(bf16[96,2048]{1,0:T(8,128)(2,1)} %get-tuple-element.8) | data formatting | bytes 786432
  124.5 1.9 %copy.23 = bf16[128,2048]{1,0:T(8,128)(2,1)} copy(bf16[128,2048]{1,0:T(8,128)(2,1)} %get-tuple-element.9) | data formatting | bytes 1048576

commit v2 on v1

--- a/solution.py
+++ b/solution.py
@@ -197,7 +197,7 @@
 
 
 def fused_fits(mesh):
-    return mesh.shape["ep"] == 4 and mesh.shape["tp"] == 4
+    return mesh.shape["grp"] == 2 and mesh.shape["ep"] == 4 and mesh.shape["tp"] == 4
 
 
 def fused_kernel(
@@ -226,7 +226,6 @@
     kbuf,
     pbuf,
     abuf,
-    bbuf,
     cbuf,
     hout,
     hbuf,
@@ -246,8 +245,10 @@
     krecv,
     asend,
     arecv,
-    bsend,
-    brecv,
+    xsend,
+    xrecv,
+    ysend,
+    yrecv,
     csend,
     crecv,
     hsend,
@@ -274,25 +275,27 @@
     dn_dev = (grp, jnp.maximum(z - 1, 0), t)
     partner_dev = (grp, z, partner)
     peer_dev = (grp, z, peer)
+    twin_dev = (1 - grp, z, t)
 
     loads = [
         pltpu.make_async_copy(ka_hbm, kbuf.at[z, :, pl.ds(0, kw)], lsem.at[0]),
         pltpu.make_async_copy(kb_hbm, kbuf.at[z, :, pl.ds(kw, kw)], lsem.at[1]),
         pltpu.make_async_copy(v_hbm, kbuf.at[z, :, pl.ds(2 * kw, vw)], lsem.at[2]),
-        pltpu.make_async_copy(gate_hbm.at[0], gate, lsem.at[3]),
-        pltpu.make_async_copy(up_hbm.at[0], up, lsem.at[4]),
-        pltpu.make_async_copy(down_hbm.at[0], down, lsem.at[5]),
-        pltpu.make_async_copy(sgate_hbm, sgate, lsem.at[6]),
-        pltpu.make_async_copy(sup_hbm, sup, lsem.at[7]),
-        pltpu.make_async_copy(sdown_hbm, sdown, lsem.at[8]),
+        pltpu.make_async_copy(gate_hbm.at[0], gate.at[0], lsem.at[3]),
+        pltpu.make_async_copy(up_hbm.at[0], up.at[0], lsem.at[4]),
+        pltpu.make_async_copy(down_hbm.at[0], down.at[0], lsem.at[5]),
+        pltpu.make_async_copy(sgate_hbm, sgate.at[0], lsem.at[6]),
+        pltpu.make_async_copy(sup_hbm, sup.at[0], lsem.at[7]),
+        pltpu.make_async_copy(sdown_hbm, sdown.at[0], lsem.at[8]),
         pltpu.make_async_copy(wo_hbm, wo, lsem.at[9]),
     ]
-    for load in loads:
+    for load in loads[3:] + loads[:3]:
         load.start()
 
     barrier = pltpu.get_barrier_semaphore()
     for other in (partner, peer, diag):
         pl.semaphore_signal(barrier, inc=1, device_id=(grp, z, other), device_id_type=MESH)
+    pl.semaphore_signal(barrier, inc=1, device_id=twin_dev, device_id_type=MESH)
 
     @pl.when(has_up)
     def _():
@@ -302,13 +305,13 @@
     def _():
         pl.semaphore_signal(barrier, inc=1, device_id=dn_dev, device_id_type=MESH)
 
-    own = z * tn + t
+    own = 2 * z + c
     wide = tokens_ref[...].astype(F32)
     scale = lax.rsqrt(jnp.mean(wide * wide, axis=-1, keepdims=True) + epsilon)
     gbuf[own] = (wide * scale * gain_ref[...]).astype(BF)
     wbuf[own] = wloc_ref[...]
 
-    pl.semaphore_wait(barrier, 3 + jnp.where(has_up, 1, 0) + jnp.where(has_dn, 1, 0))
+    pl.semaphore_wait(barrier, 4 + jnp.where(has_up, 1, 0) + jnp.where(has_dn, 1, 0))
 
     def remote(src, dst, ssem, rsem, dev):
         return pltpu.make_async_remote_copy(
@@ -346,7 +349,7 @@
         return jnp.where(z < 2, near, zn - 1 - near)
 
     def forward(k):
-        slot = k * tn + t
+        slot = 2 * k + c
 
         @pl.when(goes_up(k))
         def _():
@@ -356,8 +359,7 @@
         def _():
             gstart(slot, 1, dn_dev)
 
-        gstart(slot, 2, peer_dev)
-        gstart(slot, 3, partner_dev)
+        gstart(slot, 2, partner_dev)
 
     forward(z)
     inner = jnp.minimum(z, zn - 1 - z)
@@ -374,82 +376,109 @@
         def _():
             kcopy(k, 1, dn_dev).start()
 
-    def acopy(k, xd):
-        return remote(
-            pbuf.at[k, 2 * xd + 1 - c], abuf.at[k, xd], asend.at[k, xd], arecv.at[k, xd], partner_dev
-        )
-
-    for load in loads[3:9]:
+    def acopy(k):
+        return remote(pbuf.at[k, 1 - c], abuf.at[k], asend.at[k], arecv.at[k], partner_dev)
+
+    def cuts(buf, parts):
+        size = buf.shape[1] // (2 * parts)
+        return [(buf, (grp * parts + q) * size, (parts - grp * parts + q) * size, size) for q in range(parts)]
+
+    pieces = cuts(gate, 2) + cuts(up, 2) + cuts(down, 2) + cuts(sgate, 1) + cuts(sup, 1) + cuts(sdown, 1)
+
+    def xcopy(p):
+        buf, mine, _, size = pieces[p]
+        span = pl.ds(pl.multiple_of(mine, 16), size)
+        return remote(buf.at[0, span, :], buf.at[1, span, :], xsend.at[p], xrecv.at[p], peer_dev)
+
+    def ycopy(p):
+        buf, mine, _, size = pieces[p]
+        span = pl.ds(pl.multiple_of(mine, 16), size)
+        return remote(buf.at[1, span, :], buf.at[1, span, :], ysend.at[p], yrecv.at[p], twin_dev)
+
+    def ycopy_in(p):
+        buf, _, theirs, size = pieces[p]
+        span = pl.ds(pl.multiple_of(theirs, 16), size)
+        return remote(buf.at[1, span, :], buf.at[1, span, :], ysend.at[p], yrecv.at[p], twin_dev)
+
+    for p in range(len(pieces)):
+        if p % 2 == 0 and p < 6:
+            loads[3 + p // 2].wait()
+        if p >= 6:
+            loads[p].wait()
+        xcopy(p).start()
+    for load in loads[:3]:
         load.wait()
+
+    @pl.when(inner == 0)
+    def _():
+        kforward(z)
 
     def silu_mul(g, u):
         return (g * (1.0 / (1.0 + jnp.exp(-g))) * u).astype(BF)
 
+    def expert_part(k, side, shared):
+        rows_in = gbuf[pl.ds(2 * k, 2)].reshape(2 * rows, width)
+        g = jnp.dot(rows_in, gate[side], preferred_element_type=F32)
+        u = jnp.dot(rows_in, up[side], preferred_element_type=F32)
+        hidden = silu_mul(g, u)
+        columns = []
+        for s in range(2):
+            turned = wbuf[2 * k + s].T
+            lane = lax.broadcasted_iota(jnp.int32, turned.shape, 1)
+            columns.append(jnp.sum(jnp.where(lane == z, turned, 0.0), axis=1, keepdims=True))
+        weight = jnp.concatenate(columns, axis=0)
+        half = width // 2
+        for h in range(2):
+            span = slice(h * half, (h + 1) * half)
+            part = jnp.dot(hidden, down[side, :, span], preferred_element_type=F32) * weight
+            part = part.reshape(2, rows, half)
+            if side == 1:
+                part = part + pbuf[k, :, :, span].astype(F32)
+            pbuf[k, :, :, span] = part.astype(BF)
+
+        @pl.when(shared)
+        def _():
+            if side == 1:
+                for p in range(6, 9):
+                    ycopy_in(p).wait_recv()
+            sg = jnp.dot(rows_in, sgate[side], preferred_element_type=F32)
+            su = jnp.dot(rows_in, sup[side], preferred_element_type=F32)
+            sh = silu_mul(sg, su)
+            for h in range(2):
+                span = slice(h * half, (h + 1) * half)
+                part = jnp.dot(sh, sdown[side, :, span], preferred_element_type=F32)
+                before = pbuf[k, :, :, span].astype(F32)
+                pbuf[k, :, :, span] = (before + part.reshape(2, rows, half)).astype(BF)
+
     def gather_step(j, carry):
+        for jj, arriving in enumerate(((0, 1), (2, 3), (4, 5), (6, 7, 8))):
+
+            @pl.when(j == jj)
+            def _():
+                for p in arriving:
+                    xcopy(p).wait_recv()
+                    ycopy(p).start()
+
         for i in range(1, 4):
             when = jnp.where(inner == 1, max(i - 2, 0), i - 1)
 
             @pl.when(j == when)
             def _():
                 k = order(i)
-                gwait_recv(k * tn + t)
+                gwait_recv(2 * k + c)
                 forward(k)
                 if i == 3:
-                    for load in loads[:3]:
-                        load.wait()
-                    kforward(z)
+
+                    @pl.when(inner == 1)
+                    def _():
+                        kforward(z)
 
         k = order(j)
-        gwait_recv(k * tn + peer)
-        gstart(k * tn + peer, 3, partner_dev)
-        gwait_recv(k * tn + partner)
-        gwait_recv(k * tn + diag)
-        rows_in = gbuf[pl.ds(k * tn, tn)].reshape(tn * rows, width)
-        g = jnp.dot(rows_in, gate[...], preferred_element_type=F32)
-        u = jnp.dot(rows_in, up[...], preferred_element_type=F32)
-        hidden = silu_mul(g, u)
-        pieces = []
-        for s in range(tn):
-            turned = wbuf[k * tn + s].T
-            lane = lax.broadcasted_iota(jnp.int32, turned.shape, 1)
-            pieces.append(jnp.sum(jnp.where(lane == z, turned, 0.0), axis=1, keepdims=True))
-        weight = jnp.concatenate(pieces, axis=0)
-        half = width // 2
-        for h in range(2):
-            cols = pl.ds(h * half, half)
-            part = jnp.dot(hidden, down[:, h * half : (h + 1) * half], preferred_element_type=F32)
-            pbuf[k, :, :, cols] = (part * weight).astype(BF).reshape(tn, rows, half)
-
-        @pl.when(j == 0)
-        def _():
-            sg = jnp.dot(rows_in, sgate[...], preferred_element_type=F32)
-            su = jnp.dot(rows_in, sup[...], preferred_element_type=F32)
-            sh = silu_mul(sg, su)
-            for h in range(2):
-                cols = pl.ds(h * half, half)
-                part = jnp.dot(sh, sdown[:, h * half : (h + 1) * half], preferred_element_type=F32)
-                before = pbuf[k, :, :, cols].astype(F32)
-                pbuf[k, :, :, cols] = (before + part.reshape(tn, rows, half)).astype(BF)
-
-        for xd in range(2):
-            acopy(k, xd).start()
+        gwait_recv(2 * k + 1 - c)
+        expert_part(k, 0, j == 0)
         return carry
 
     lax.fori_loop(0, zn, gather_step, 0)
-
-    def bcopy(k):
-        return remote(pbuf.at[k, peer], bbuf.at[k], bsend.at[k], brecv.at[k], peer_dev)
-
-    def pair_step(i, carry):
-        k = order(zn - 1 - i)
-        acopy(k, 0).wait_recv()
-        acopy(k, 1).wait_recv()
-        pbuf[k, peer] = (pbuf[k, peer].astype(F32) + abuf[k, 1 - x].astype(F32)).astype(BF)
-        bcopy(k).start()
-        pbuf[k, t] = (pbuf[k, t].astype(F32) + abuf[k, x].astype(F32)).astype(BF)
-        return carry
-
-    lax.fori_loop(0, zn, pair_step, 0)
 
     def key_step(j, carry):
         k = order(j)
@@ -457,7 +486,50 @@
         kforward(k)
         return carry
 
-    lax.fori_loop(1, zn, key_step, 0)
+    @pl.when(inner == 1)
+    def _():
+        lax.fori_loop(1, zn, key_step, 0)
+
+    for p in range(6):
+        ycopy_in(p).wait_recv()
+
+    def ccopy(k, h, way, dev):
+        span = pl.ds(h * (rows // 2), rows // 2)
+        return remote(
+            pbuf.at[k, c, span, :], cbuf.at[way, k, span, :], csend.at[k, h], crecv.at[way, k, h], dev
+        )
+
+    def pair_sum(k):
+        acopy(k).wait_recv()
+        for h in range(2):
+            span = pl.ds(h * (rows // 2), rows // 2)
+            pbuf[k, c, span, :] = (pbuf[k, c, span, :].astype(F32) + abuf[k, span, :].astype(F32)).astype(BF)
+
+            @pl.when(jnp.logical_and(z == 0, k > z))
+            def _():
+                ccopy(k, h, 0, up_dev).start()
+
+            @pl.when(jnp.logical_and(z == zn - 1, k < z))
+            def _():
+                ccopy(k, h, 1, dn_dev).start()
+
+    def finish_step(i, carry):
+        k = order(zn - 1 - i)
+        expert_part(k, 1, i == zn - 1)
+        acopy(k).start()
+
+        @pl.when(i > 0)
+        def _():
+            pair_sum(order(zn - i))
+
+        return carry
+
+    lax.fori_loop(0, zn, finish_step, 0)
+    pair_sum(z)
+
+    @pl.when(inner == 0)
+    def _():
+        lax.fori_loop(1, zn, key_step, 0)
 
     heads = vw // hgain_ref.shape[1]
     head = kw // heads
@@ -508,31 +580,26 @@
         hcopy(other).start()
     hbuf[t] = hout[pl.ds(pl.multiple_of(t * orow, 16), orow), :]
 
-    def ccopy(k, way, dev):
-        return remote(pbuf.at[k, t], cbuf.at[way, k], csend.at[k], crecv.at[way, k], dev)
-
     def line_step(i, carry):
         k = order(zn - 1 - i)
-        bcopy(k).wait_recv()
-        pbuf[k, t] = (pbuf[k, t].astype(F32) + bbuf[k].astype(F32)).astype(BF)
-
-        @pl.when(k > z)
-        def _():
-            @pl.when(has_dn)
+        for h in range(2):
+            span = pl.ds(h * (rows // 2), rows // 2)
+
+            @pl.when(jnp.logical_and(k > z, has_dn))
             def _():
-                ccopy(k, 0, up_dev).wait_recv()
-                pbuf[k, t] = (pbuf[k, t].astype(F32) + cbuf[0, k].astype(F32)).astype(BF)
-
-            ccopy(k, 0, up_dev).start()
-
-        @pl.when(k < z)
-        def _():
-            @pl.when(has_up)
+                ccopy(k, h, 0, up_dev).wait_recv()
+                pbuf[k, c, span, :] = (
+                    pbuf[k, c, span, :].astype(F32) + cbuf[0, k, span, :].astype(F32)
+                ).astype(BF)
+                ccopy(k, h, 0, up_dev).start()
+
+            @pl.when(jnp.logical_and(k < z, has_up))
             def _():
-                ccopy(k, 1, dn_dev).wait_recv()
-                pbuf[k, t] = (pbuf[k, t].astype(F32) + cbuf[1, k].astype(F32)).astype(BF)
-
-            ccopy(k, 1, dn_dev).start()
+                ccopy(k, h, 1, dn_dev).wait_recv()
+                pbuf[k, c, span, :] = (
+                    pbuf[k, c, span, :].astype(F32) + cbuf[1, k, span, :].astype(F32)
+                ).astype(BF)
+                ccopy(k, h, 1, dn_dev).start()
 
         return carry
 
@@ -550,23 +617,27 @@
             )
         mixed_ref[:, h * half : (h + 1) * half] = acc.astype(BF)
 
-    bcopy(z).wait_recv()
-    pbuf[z, t] = (pbuf[z, t].astype(F32) + bbuf[z].astype(F32)).astype(BF)
-
-    @pl.when(has_dn)
-    def _():
-        ccopy(z, 0, up_dev).wait_recv()
-        pbuf[z, t] = (pbuf[z, t].astype(F32) + cbuf[0, z].astype(F32)).astype(BF)
-
-    @pl.when(has_up)
-    def _():
-        ccopy(z, 1, dn_dev).wait_recv()
-        pbuf[z, t] = (pbuf[z, t].astype(F32) + cbuf[1, z].astype(F32)).astype(BF)
-
-    out_ref[...] = pbuf[z, t]
+    for h in range(2):
+        span = pl.ds(h * (rows // 2), rows // 2)
+
+        @pl.when(has_dn)
+        def _():
+            ccopy(z, h, 0, up_dev).wait_recv()
+            pbuf[z, c, span, :] = (
+                pbuf[z, c, span, :].astype(F32) + cbuf[0, z, span, :].astype(F32)
+            ).astype(BF)
+
+        @pl.when(has_up)
+        def _():
+            ccopy(z, h, 1, dn_dev).wait_recv()
+            pbuf[z, c, span, :] = (
+                pbuf[z, c, span, :].astype(F32) + cbuf[1, z, span, :].astype(F32)
+            ).astype(BF)
+
+    out_ref[...] = pbuf[z, c]
 
     def drain_step(k, carry):
-        slot = k * tn + t
+        slot = 2 * k + c
 
         @pl.when(goes_up(k))
         def _():
@@ -578,19 +649,19 @@
             gwait_send(slot, 1, dn_dev)
             kcopy(k, 1, dn_dev).wait_send()
 
-        gwait_send(slot, 2, peer_dev)
-        gwait_send(slot, 3, partner_dev)
-        gwait_send(k * tn + peer, 3, partner_dev)
-        for xd in range(2):
-            acopy(k, xd).wait_send()
-        bcopy(k).wait_send()
+        gwait_send(slot, 2, partner_dev)
+        acopy(k).wait_send()
 
         @pl.when(k != z)
         def _():
-            ccopy(k, 0, up_dev).wait_send()
+            for h in range(2):
+                ccopy(k, h, 0, up_dev).wait_send()
 
         return carry
 
+    for p in range(len(pieces)):
+        xcopy(p).wait_send()
+        ycopy(p).wait_send()
     lax.fori_loop(0, zn, drain_step, 0)
     for other in (partner, peer, diag):
         hcopy(other).wait_send()
@@ -630,7 +701,7 @@
     smem = pl.BlockSpec(memory_space=pltpu.SMEM)
     hbm = pl.BlockSpec(memory_space=pltpu.HBM)
     dma = pltpu.SemaphoreType.DMA
-    slots = zn * tn
+    slots = zn * 2
     hidden = expert_gate.shape[2]
     shared = shared_gate.shape[1]
     mixed, expert_out = pl.pallas_call(
@@ -645,32 +716,33 @@
             pltpu.VMEM((slots, rows, width), BF),
             pltpu.VMEM((slots, pad, rows), F32),
             pltpu.VMEM((zn, arow, 2 * kw + vw), BF),
-            pltpu.VMEM((zn, tn, rows, width), BF),
             pltpu.VMEM((zn, 2, rows, width), BF),
             pltpu.VMEM((zn, rows, width), BF),
             pltpu.VMEM((2, zn, rows, width), BF),
             pltpu.VMEM((arow, vw), BF),
             pltpu.VMEM((tn, arow // tn, vw), BF),
-            pltpu.VMEM((width, hidden), BF),
-            pltpu.VMEM((width, hidden), BF),
-            pltpu.VMEM((hidden, width), BF),
-            pltpu.VMEM((width, shared), BF),
-            pltpu.VMEM((width, shared), BF),
-            pltpu.VMEM((shared, width), BF),
+            pltpu.VMEM((2, width, hidden), BF),
+            pltpu.VMEM((2, width, hidden), BF),
+            pltpu.VMEM((2, hidden, width), BF),
+            pltpu.VMEM((2, width, shared), BF),
+            pltpu.VMEM((2, width, shared), BF),
+            pltpu.VMEM((2, shared, width), BF),
             pltpu.VMEM(out_weight.shape, BF),
             dma((10,)),
-            dma((4, slots)),
+            dma((3, slots)),
             dma((slots,)),
-            dma((4, slots)),
+            dma((3, slots)),
             dma((slots,)),
             dma((2, zn)),
             dma((zn,)),
-            dma((zn, 2)),
-            dma((zn, 2)),
             dma((zn,)),
             dma((zn,)),
-            dma((zn,)),
-            dma((2, zn)),
+            dma((9,)),
+            dma((9,)),
+            dma((9,)),
+            dma((9,)),
+            dma((zn, 2)),
+            dma((2, zn, 2)),
             dma((tn,)),
             dma((tn,)),
         ],

time: 129 us -> 113 us (0.88); the launches traced: 126 us -> 113 us
  Pallas kernels: 120 us -> 107 us
    pallas_call x1, Pallas kernels: 120 us -> 107 us  [fused_shards(): pl.pallas_call(functools.partial(fused_kernel, zn), out_shape=(jax.ShapeD...]
where the time goes in v2:
time: 113 us
  Pallas kernels  107 us (95%)
  local copies, waits for them, and re-layouts  5.16 us (5%)
    pallas_call x1, Pallas kernels, fused_shards(): pl.pallas_call(functools.partial(fused_kernel, zn), out_shape=(jax.ShapeD...  107 us
    unnamed x2, local copies, waits for them, and re-layouts  3.65 us

profile of v2, /device:TPU:8, one launch (start us, length us, event | category | flops | bytes accessed | tf_op | source)
XLA Modules:
  0.0 113.1 jit_solution(10065180537032573120)
XLA Ops:
  0.6 0.8 slice_bitcast_fusion.3
  1.4 0.8 slice_bitcast_fusion.2
  2.1 0.6 select_add_fusion.wloc_ref
  2.7 106.7 %shard_map.185 = (bf16[96,2048]{1,0:T(8,128)(2,1)}, bf16[128,2048]{1,0:T(8,128)(2,1)}) custom-call(bf16[128,2048]{1,0:T(8,128)(2,1)} %tokens_ref.1, f32[1,2048]{1,0:T(1,128)} %bitcast.11, f32[8,128]{1,0:T(8,128)} %select_add_fusion.wloc_ref, bf16[384,128]{1,0:T(8,128)(2,1)} %qa_ref.1, bf16[384,128]{1,0:T(8,128)(2,1)} %qb_ref.1, bf16[384,128]{1,0:T(8,128)(2,1)} %ka_hbm.1, ...), custom_call_target="tpu_custom_call" | custom-call | tf_op jit(solution)/shard_map/pallas_call | solution.py:707
  109.5 1.8 %copy.22 = bf16[96,2048]{1,0:T(8,128)(2,1)} copy(bf16[96,2048]{1,0:T(8,128)(2,1)} %get-tuple-element.8) | data formatting | bytes 786432
  111.3 1.9 %copy.23 = bf16[128,2048]{1,0:T(8,128)(2,1)} copy(bf16[128,2048]{1,0:T(8,128)(2,1)} %get-tuple-element.9) | data formatting | bytes 1048576

commit v3 on v2

--- a/solution.py
+++ b/solution.py
@@ -383,7 +383,7 @@
         size = buf.shape[1] // (2 * parts)
         return [(buf, (grp * parts + q) * size, (parts - grp * parts + q) * size, size) for q in range(parts)]
 
-    pieces = cuts(gate, 2) + cuts(up, 2) + cuts(down, 2) + cuts(sgate, 1) + cuts(sup, 1) + cuts(sdown, 1)
+    pieces = cuts(gate, 2) + cuts(up, 2) + cuts(down, 4) + cuts(sgate, 1) + cuts(sup, 1) + cuts(sdown, 1)
 
     def xcopy(p):
         buf, mine, _, size = pieces[p]
@@ -401,10 +401,10 @@
         return remote(buf.at[1, span, :], buf.at[1, span, :], ysend.at[p], yrecv.at[p], twin_dev)
 
     for p in range(len(pieces)):
-        if p % 2 == 0 and p < 6:
+        if p in (0, 2, 4):
             loads[3 + p // 2].wait()
-        if p >= 6:
-            loads[p].wait()
+        if p >= 8:
+            loads[p - 2].wait()
         xcopy(p).start()
     for load in loads[:3]:
         load.wait()
@@ -439,7 +439,7 @@
         @pl.when(shared)
         def _():
             if side == 1:
-                for p in range(6, 9):
+                for p in range(8, 11):
                     ycopy_in(p).wait_recv()
             sg = jnp.dot(rows_in, sgate[side], preferred_element_type=F32)
             su = jnp.dot(rows_in, sup[side], preferred_element_type=F32)
@@ -451,7 +451,7 @@
                 pbuf[k, :, :, span] = (before + part.reshape(2, rows, half)).astype(BF)
 
     def gather_step(j, carry):
-        for jj, arriving in enumerate(((0, 1), (2, 3), (4, 5), (6, 7, 8))):
+        for jj, arriving in enumerate(((0, 1), (2, 3), (4, 5, 6, 7), (8, 9, 10))):
 
             @pl.when(j == jj)
             def _():
@@ -490,19 +490,19 @@
     def _():
         lax.fori_loop(1, zn, key_step, 0)
 
-    for p in range(6):
+    for p in range(8):
         ycopy_in(p).wait_recv()
 
     def ccopy(k, h, way, dev):
-        span = pl.ds(h * (rows // 2), rows // 2)
+        span = pl.ds(h * (rows // 4), rows // 4)
         return remote(
             pbuf.at[k, c, span, :], cbuf.at[way, k, span, :], csend.at[k, h], crecv.at[way, k, h], dev
         )
 
     def pair_sum(k):
         acopy(k).wait_recv()
-        for h in range(2):
-            span = pl.ds(h * (rows // 2), rows // 2)
+        for h in range(4):
+            span = pl.ds(h * (rows // 4), rows // 4)
             pbuf[k, c, span, :] = (pbuf[k, c, span, :].astype(F32) + abuf[k, span, :].astype(F32)).astype(BF)
 
             @pl.when(jnp.logical_and(z == 0, k > z))
@@ -558,7 +558,6 @@
             hout[pl.ds(r, qrows), h * vdim : (h + 1) * vdim] = (mix * norm * hgain_ref[...]).astype(BF)
         return carry
 
-    lax.fori_loop(0, 3, attend_step, 0)
 
     orow = arow // tn
 
@@ -576,14 +575,10 @@
             hout.at[pl.ds(0, orow), :], hbuf.at[src], hsend.at[src], hrecv.at[src], (grp, z, src)
         ).wait_recv()
 
-    for other in (peer, diag, partner):
-        hcopy(other).start()
-    hbuf[t] = hout[pl.ds(pl.multiple_of(t * orow, 16), orow), :]
-
     def line_step(i, carry):
-        k = order(zn - 1 - i)
-        for h in range(2):
-            span = pl.ds(h * (rows // 2), rows // 2)
+        k = order(jnp.where(i == 0, zn - 1, i))
+        for h in range(4):
+            span = pl.ds(h * (rows // 4), rows // 4)
 
             @pl.when(jnp.logical_and(k > z, has_dn))
             def _():
@@ -600,6 +595,14 @@
                     pbuf[k, c, span, :].astype(F32) + cbuf[1, k, span, :].astype(F32)
                 ).astype(BF)
                 ccopy(k, h, 1, dn_dev).start()
+
+        lax.fori_loop(jnp.where(i == 0, 0, 1), jnp.where(i == 0, 1, jnp.where(i == 1, 3, 1)), attend_step, 0)
+
+        @pl.when(i == 1)
+        def _():
+            for other in (peer, diag, partner):
+                hcopy(other).start()
+            hbuf[t] = hout[pl.ds(pl.multiple_of(t * orow, 16), orow), :]
 
         return carry
 
@@ -617,8 +620,8 @@
             )
         mixed_ref[:, h * half : (h + 1) * half] = acc.astype(BF)
 
-    for h in range(2):
-        span = pl.ds(h * (rows // 2), rows // 2)
+    for h in range(4):
+        span = pl.ds(h * (rows // 4), rows // 4)
 
         @pl.when(has_dn)
         def _():
@@ -654,7 +657,7 @@
 
         @pl.when(k != z)
         def _():
-            for h in range(2):
+            for h in range(4):
                 ccopy(k, h, 0, up_dev).wait_send()
 
         return carry
@@ -737,12 +740,12 @@
             dma((zn,)),
             dma((zn,)),
             dma((zn,)),
-            dma((9,)),
-            dma((9,)),
-            dma((9,)),
-            dma((9,)),
-            dma((zn, 2)),
-            dma((2, zn, 2)),
+            dma((11,)),
+            dma((11,)),
+            dma((11,)),
+            dma((11,)),
+            dma((zn, 4)),
+            dma((2, zn, 4)),
             dma((tn,)),
             dma((tn,)),
         ],

time: 113 us -> 113 us (level)
  no operation moved by 1% of the time
where the time goes in v3:
time: 113 us
  Pallas kernels  107 us (95%)
  local copies, waits for them, and re-layouts  5.16 us (5%)
    pallas_call x1, Pallas kernels, fused_shards(): pl.pallas_call(functools.partial(fused_kernel, zn), out_shape=(jax.ShapeD...  107 us
    unnamed x2, local copies, waits for them, and re-layouts  3.65 us

profile of v3, /device:TPU:8, one launch (start us, length us, event | category | flops | bytes accessed | tf_op | source)
XLA Modules:
  0.0 113.0 jit_solution(15133790062273704221)
XLA Ops:
  0.6 0.8 slice_bitcast_fusion.3
  1.4 0.8 slice_bitcast_fusion.2
  2.1 0.6 select_add_fusion.wloc_ref
  2.7 106.6 %shard_map.185 = (bf16[96,2048]{1,0:T(8,128)(2,1)}, bf16[128,2048]{1,0:T(8,128)(2,1)}) custom-call(bf16[128,2048]{1,0:T(8,128)(2,1)} %tokens_ref.1, f32[1,2048]{1,0:T(1,128)} %bitcast.11, f32[8,128]{1,0:T(8,128)} %select_add_fusion.wloc_ref, bf16[384,128]{1,0:T(8,128)(2,1)} %qa_ref.1, bf16[384,128]{1,0:T(8,128)(2,1)} %qb_ref.1, bf16[384,128]{1,0:T(8,128)(2,1)} %ka_hbm.1, ...), custom_call_target="tpu_custom_call" | custom-call | tf_op jit(solution)/shard_map/pallas_call | solution.py:710
  109.4 1.8 %copy.22 = bf16[96,2048]{1,0:T(8,128)(2,1)} copy(bf16[96,2048]{1,0:T(8,128)(2,1)} %get-tuple-element.8) | data formatting | bytes 786432
  111.2 1.9 %copy.23 = bf16[128,2048]{1,0:T(8,128)(2,1)} copy(bf16[128,2048]{1,0:T(8,128)(2,1)} %get-tuple-element.9) | data formatting | bytes 1048576

commit v4 on v3

--- a/solution.py
+++ b/solution.py
@@ -451,7 +451,7 @@
                 pbuf[k, :, :, span] = (before + part.reshape(2, rows, half)).astype(BF)
 
     def gather_step(j, carry):
-        for jj, arriving in enumerate(((0, 1), (2, 3), (4, 5, 6, 7), (8, 9, 10))):
+        for jj, arriving in enumerate(((0, 1), (2, 3), (4, 5, 6, 7))):
 
             @pl.when(j == jj)
             def _():
@@ -515,6 +515,13 @@
 
     def finish_step(i, carry):
         k = order(zn - 1 - i)
+
+        @pl.when(i == zn - 2)
+        def _():
+            for p in range(8, 11):
+                xcopy(p).wait_recv()
+                ycopy(p).start()
+
         expert_part(k, 1, i == zn - 1)
         acopy(k).start()
 

time: 113 us -> 116 us (1.027)
  Pallas kernels: 107 us -> 109 us
    pallas_call x1, Pallas kernels: 107 us -> 109 us  [fused_shards(): pl.pallas_call(functools.partial(fused_kernel, zn), out_shape=(jax.ShapeD...]
where the time goes in v4:
time: 116 us
  Pallas kernels  109 us (94%)
  local copies, waits for them, and re-layouts  5.16 us (4%)
    pallas_call x1, Pallas kernels, fused_shards(): pl.pallas_call(functools.partial(fused_kernel, zn), out_shape=(jax.ShapeD...  109 us
    unnamed x2, local copies, waits for them, and re-layouts  3.65 us

profile of v4, /device:TPU:8, one launch (start us, length us, event | category | flops | bytes accessed | tf_op | source)
XLA Modules:
  0.0 115.5 jit_solution(8124496152560821370)
XLA Ops:
  0.6 0.8 slice_bitcast_fusion.3
  1.4 0.8 slice_bitcast_fusion.2
  2.1 0.6 select_add_fusion.wloc_ref
  2.7 109.1 %shard_map.185 = (bf16[96,2048]{1,0:T(8,128)(2,1)}, bf16[128,2048]{1,0:T(8,128)(2,1)}) custom-call(bf16[128,2048]{1,0:T(8,128)(2,1)} %tokens_ref.1, f32[1,2048]{1,0:T(1,128)} %bitcast.11, f32[8,128]{1,0:T(8,128)} %select_add_fusion.wloc_ref, bf16[384,128]{1,0:T(8,128)(2,1)} %qa_ref.1, bf16[384,128]{1,0:T(8,128)(2,1)} %qb_ref.1, bf16[384,128]{1,0:T(8,128)(2,1)} %ka_hbm.1, ...), custom_call_target="tpu_custom_call" | custom-call | tf_op jit(solution)/shard_map/pallas_call | solution.py:717
  111.9 1.8 %copy.22 = bf16[96,2048]{1,0:T(8,128)(2,1)} copy(bf16[96,2048]{1,0:T(8,128)(2,1)} %get-tuple-element.8) | data formatting | bytes 786432
  113.7 1.9 %copy.23 = bf16[128,2048]{1,0:T(8,128)(2,1)} copy(bf16[128,2048]{1,0:T(8,128)(2,1)} %get-tuple-element.9) | data formatting | bytes 1048576
